TPU v7x, 32 devices: a whole 2x2x4 slice. The times are simulated.
32 devices in a mesh: fs: 8 (over z, y), tp: 4 (over x, core).
Axes of the slice: x: 2, y: 2, z: 4, core: 2. Of those that a mesh axis runs over, the one named last changes fastest.
Arguments:
- prompt: bfloat16 [6144, 2048], P('fs'), may hold values from -6 to 6
- routes: int32 [6144, 2], P('fs'), may hold values from 0 to 15, all different within a row; in each aligned block of 768 rows (0 to 767, 768 to 1535, ...) at most 192 rows name the same one
- affinity: float32 [6144, 2], P('fs'), may hold values from 0.05 to 1
- norm_gain: float32 [2048], P('fs'), may hold values from 0.1 to 1.9
- gate_master: float32 [16, 2048, 1024], P(None, 'fs', 'tp'), may hold values from -0.125 to 0.125
- up_master: float32 [16, 2048, 1024], P(None, 'fs', 'tp'), may hold values from -0.125 to 0.125
- down_master: float32 [16, 1024, 2048], P(None, 'fs', 'tp'), may hold values from -0.1875 to 0.1875
Outputs:
- mixed: bfloat16 [6144, 2048], P('fs', 'tp')
- gate_weights: bfloat16 [16, 2048, 1024], P('fs', None, 'tp')
- up_weights: bfloat16 [16, 2048, 1024], P('fs', None, 'tp')
- down_weights: bfloat16 [16, 1024, 2048], P('fs', None, 'tp')
Inputs may be any that keep to these rules, and one draw needn't show every extreme that they name: `routes`: each row names 2 different experts. In each aligned block of 768 rows no expert is named more than 192 times, a bound that some block reaches.
All inputs are finite; a program needn't handle non-finite values.
Results may differ from a plain program's by a relative error of at most 0.0086.
Values may be sent and summed in bfloat16 or wider, within the bound.
A program may use at most 128 MiB of HBM per device.

v0:
```python
import jax
import jax.numpy as jnp
from jax import lax
from jax.sharding import PartitionSpec as P

norm_eps = 1e-06


def per_device(prompt, routes, affinity, norm_gain, gate_master, up_master, down_master):
    tp_count = lax.axis_size("tp")
    experts = gate_master.shape[0]
    gain_rows = norm_gain[None, :, None]
    gate_half = (gate_master * gain_rows).astype(jnp.bfloat16)
    up_half = (up_master * gain_rows).astype(jnp.bfloat16)
    down_half = down_master.astype(jnp.bfloat16)
    gate_new, up_new, down_new = (
        lax.all_to_all(gate_half, "fs", split_axis=0, concat_axis=1, tiled=True),
        lax.all_to_all(up_half, "fs", split_axis=0, concat_axis=1, tiled=True),
        lax.all_to_all(down_half, "fs", split_axis=0, concat_axis=1, tiled=True),
    )
    token_count = prompt.shape[0]
    top_count = routes.shape[1]
    model_width = prompt.shape[1]
    capacity = 2 * token_count * top_count // experts
    flat_ids = routes.reshape(-1)
    onehot = (flat_ids[:, None] == jnp.arange(experts, dtype=jnp.int32)[None, :]).astype(jnp.int32)
    slot_rank = jnp.sum(jnp.cumsum(onehot, axis=0) * onehot, axis=1) - 1
    slot_index = flat_ids * capacity + slot_rank
    values = prompt.astype(jnp.float32)
    normed = (
        values * lax.rsqrt(jnp.mean(values * values, axis=-1, keepdims=True) + norm_eps)
    ).astype(jnp.bfloat16)
    column_width = model_width // tp_count
    column_slice = lax.dynamic_slice_in_dim(
        normed, lax.axis_index("tp") * column_width, column_width, 1
    )
    slot_rows = jnp.broadcast_to(
        column_slice[:, None, :], (token_count, top_count, column_width)
    ).reshape(-1, column_width)
    outbox = (
        jnp.zeros((experts * capacity, column_width), jnp.bfloat16).at[slot_index].set(slot_rows)
    )
    received = lax.all_to_all(
        outbox.reshape(experts, capacity, column_width),
        "fs",
        split_axis=0,
        concat_axis=1,
        tiled=True,
    )
    shard_piece = lax.all_gather(received, "tp", axis=2, tiled=True)
    gate_pre = jnp.einsum("erd,edf->erf", shard_piece, gate_new, preferred_element_type=jnp.float32)
    up_pre = jnp.einsum("erd,edf->erf", shard_piece, up_new, preferred_element_type=jnp.float32)
    hidden = (jax.nn.silu(gate_pre) * up_pre).astype(jnp.bfloat16)
    expert_out = jnp.einsum(
        "erf,efd->erd",
        lax.all_gather(hidden, "tp", axis=2, tiled=True),
        down_new,
        preferred_element_type=jnp.float32,
    ).astype(jnp.bfloat16)
    returned = lax.all_to_all(expert_out, "fs", split_axis=1, concat_axis=0, tiled=True)
    picked = returned.reshape(experts * capacity, -1)[slot_index].reshape(
        token_count, top_count, -1
    )
    share = affinity / jnp.sum(affinity, axis=1, keepdims=True)
    mixed_out = jnp.sum(share[:, :, None] * picked.astype(jnp.float32), axis=1).astype(jnp.bfloat16)
    return (mixed_out, gate_new, up_new, down_new)


def solution(mesh):
    in_specs = (
        P("fs", None),
        P("fs", None),
        P("fs", None),
        P("fs"),
        P(None, "fs", "tp"),
        P(None, "fs", "tp"),
        P(None, "fs", "tp"),
    )
    out_specs = (P("fs", "tp"), P("fs", None, "tp"), P("fs", None, "tp"), P("fs", None, "tp"))
    return jax.shard_map(
        per_device, mesh=mesh, in_specs=in_specs, out_specs=out_specs, check_vma=False
    )
```

profile of v0, /device:TPU:0, one launch (start us, length us, event | category | flops | bytes accessed | tf_op | source)
XLA Modules:
  0.0 415.7 jit_solution(1486511476478039766)
XLA Ops:
  7.2 0.0 all-gather.3.cloned.1.call-start
  7.2 0.7 broadcast_multiply_fusion
  7.9 0.9 copy.27
  8.8 0.2 eq.29
  9.0 0.2 eq.25
  9.2 0.0 copy-start.1
  9.2 5.5 %convert_element_type.36 = f32[768,2048]{1,0:T(8,128)} convert(bf16[768,2048]{1,0:T(8,128)(2,1)} %param.7) | non-fusion elementwise | flops 1572864 | bytes 9437184 | tf_op jit(solution)/shard_map/convert_element_type | solution.py:29
  14.8 0.7 multiply_reduce_fusion
  15.5 0.2 copy.26
  15.7 0.3 mul.65
  15.9 4.5 %reduce-window.6 = s32[16,12,128]{2,1,0:T(8,128)S(1)} reduce-window(s32[16,12,128]{2,1,0:T(8,128)S(1)} %fusion.4, s32[]{:T(128)} %constant.15.clone.1), window={size=1x1x128 pad=0_0x0_0x127_0}, to_apply=%region_1.2 | reduce-window | flops 3121152 | bytes 196612 | tf_op jit(solution)/shard_map/reduce-window
  20.5 0.4 slice_reduce_fusion
  20.9 0.2 reduce-window.9
  21.1 0.1 broadcast_add_fusion
  21.3 1.6 fusion.1
  22.9 0.8 broadcast_in_dim.5
  23.7 2.0 reshape.101
  25.7 8.8 %scatter_custom_fusion = bf16[3072,512]{1,0:T(8,128)(2,1)S(1)} fusion(s32[1536]{0:T(1024)S(1)} %fusion.7, bf16[1536,512]{1,0:T(8,128)(2,1)} %reshape.101, bf16[]{:T(256)} %constant.13.clone.1), kind=kCustom, calls=%fused_computation.11 | custom fusion | bytes 3146240 | tf_op jit(solution)/shard_map/scatter | solution.py:41
  34.6 77.8 %all_to_all.87 = bf16[16,192,512]{2,1,0:T(8,128)(2,1)S(1)} all-to-all(bf16[16,192,512]{2,1,0:T(8,128)(2,1)S(1)} %bitcast.44), channel_id=1, replica_groups=mesh['fs'=8,'tp'=4] {'fs'}, dimensions={0} | all-to-all | bytes 6291456 | tf_op jit(solution)/shard_map/all_to_all | solution.py:43
  112.4 1.9 copy.29
  114.4 0.0 all-gather.3.cloned.1.call-update
  114.4 0.7 copy-done.5
  115.0 5.8 %multiply_convert_fusion.1 = (bf16[16,256,256]{2,1,0:T(8,128)(2,1)}, bf16[16,256,256]{2,1,0:T(8,128)(2,1)S(1)}) fusion(f32[16,256,256]{2,1,0:T(8,128)} %param.11, f32[256]{0:T(256)S(1)} %copy-done.5, f32[16,256,256]{2,1,0:T(8,128)} %param.12), kind=kLoop, calls=%fused_computation.4 | loop fusion | flops 4194304 | bytes 12583936 | tf_op jit(solution)/shard_map/convert_element_type | solution.py:13
  120.8 51.5 %all_to_all.88 = bf16[16,256,256]{2,1,0:T(8,128)(2,1)} all-to-all(bf16[16,256,256]{2,1,0:T(8,128)(2,1)S(1)} %get-tuple-element.5), channel_id=1, replica_groups=mesh['fs'=8,'tp'=4] {'fs'}, dimensions={0} | all-to-all | bytes 4194304 | tf_op jit(solution)/shard_map/all_to_all | solution.py:18
  172.3 3.6 all-to-all-start.1
  175.9 0.2 all-gather.5.cloned.1.call-start
  176.2 3.1 copy.31
  179.2 44.4 %all-to-all-done.1 = bf16[16,256,256]{2,1,0:T(8,128)(2,1)S(1)} async-done(((bf16[16,256,256]{2,1,0:T(8,128)(2,1)}), bf16[16,256,256]{2,1,0:T(8,128)(2,1)S(1)}, u32[]{:S(2)}, u32[]{:S(2)}) %all-to-all-start.1) | async-done | bytes 2097184 | tf_op jit(solution)/shard_map/all_to_all | solution.py:17
  223.6 1.5 copy.30
  225.1 7.2 %fusion.8 = f32[2,1536,256]{2,1,0:T(8,128)S(1)} fusion(bf16[2,1536,2048]{2,1,0:T(8,128)(2,1)} %all-gather.3.cloned.1.call-done, bf16[2,2048,256]{2,1,0:T(8,128)(2,1)} %bitcast.51), kind=kOutput, calls=%fused_computation.28 | convolution fusion | flops 3221225472 | bytes 17825792 | tf_op jit(solution)/shard_map/erd,edf->erf/dot_general | solution.py:51
  232.3 2.2 copy-done.6
  234.5 5.0 %fusion = bf16[2,1536,256]{2,1,0:T(8,128)(2,1)} fusion(bf16[2,1536,2048]{2,1,0:T(8,128)(2,1)S(1)} %copy-done.6, bf16[2,2048,256]{2,1,0:T(8,128)(2,1)S(1)} %bitcast.50, f32[2,1536,256]{2,1,0:T(8,128)S(1)} %fusion.8), kind=kOutput, calls=%fused_computation.8 | convolution fusion | flops 3225944064 | bytes 19398656 | tf_op jit(solution)/shard_map/erd,edf->erf/dot_general | solution.py:52
  239.6 0.0 all-gather.5.cloned.1.call-update
  239.6 2.5 convert_element_type.41
  242.1 51.8 %all_to_all.89 = bf16[16,128,512]{2,1,0:T(8,128)(2,1)S(1)} all-to-all(bf16[16,128,512]{2,1,0:T(8,128)(2,1)S(1)} %convert_element_type.41), channel_id=1, replica_groups=mesh['fs'=8,'tp'=4] {'fs'}, dimensions={0} | all-to-all | bytes 4194304 | tf_op jit(solution)/shard_map/all_to_all | solution.py:19
  293.9 0.2 copy.32
  294.1 0.0 copy-start.3
  294.1 0.0 all-gather.5.cloned.1.call-done
  294.1 7.3 %convolution_convert_fusion = bf16[2,1536,512]{2,1,0:T(8,128)(2,1)S(1)} fusion(bf16[2,1536,1024]{2,1,0:T(8,128)(2,1)} %all-gather.5.cloned.1.call-done, bf16[2,1024,512]{2,1,0:T(8,128)(2,1)S(1)} %bitcast.53), kind=kOutput, calls=%fused_computation.5 | convolution fusion | flops 3222798336 | bytes 11534336 | tf_op jit(solution)/shard_map/erf,efd->erd/dot_general | solution.py:54
  301.4 14.5 %copy.33 = bf16[2,1536,512]{2,0,1:T(2,128)(2,1)} copy(bf16[2,1536,512]{2,1,0:T(8,128)(2,1)S(1)} %convolution_convert_fusion) | data formatting | bytes 6291456 | tf_op jit(solution)/shard_map/convert_element_type | solution.py:59
  315.9 4.0 all-to-all-start.4
  320.0 0.2 copy.25
  320.2 70.0 %all-to-all-done.4 = bf16[2,1536,512]{2,0,1:T(2,128)(2,1)S(1)} async-done(((bf16[2,1536,512]{2,0,1:T(2,128)(2,1)}), bf16[2,1536,512]{2,0,1:T(2,128)(2,1)S(1)}, u32[]{:S(2)}, u32[]{:S(2)}) %all-to-all-start.4) | async-done | bytes 3145760 | tf_op jit(solution)/shard_map/all_to_all | solution.py:60
  390.2 1.7 copy-done
  391.8 2.5 copy.34
  394.3 5.4 %gather_fusion = bf16[1536,512]{1,0:T(8,128)(2,1)} fusion(bf16[3072,512]{1,0:T(8,128)(2,1)S(1)} %bitcast.41, s32[2048]{0:T(1024)S(1)} %pad_clamp_fusion), kind=kCustom, calls=%fused_computation | custom fusion | bytes 3151872 | tf_op jit(solution)/shard_map/gather | solution.py:61
  399.8 3.4 reshape.88
  403.2 5.7 %multiply_reduce_fusion.1 = bf16[768,512]{1,0:T(8,128)(2,1)} fusion(f32[768,2,512]{2,1,0:T(2,128)S(1)} %reshape.88, f32[768,2]{1,0:T(8,128)S(1)} %copy.25), kind=kLoop, calls=%fused_computation.7 | loop fusion | flops 1179648 | bytes 3938304 | tf_op jit(solution)/shard_map/reduce_sum | solution.py:65
  (18 shorter events, 0.1 us)
Async XLA Ops:
  7.2 217.9 %all-gather.3.cloned.1.call-start = ((), (), s32[]{:S(2)}) async-start(), calls=%async_computation.5 | async-start | bytes 15728640 | tf_op jit(solution)/shard_map/all_gather | solution.py:50
  9.2 5.6 %copy-start.1 = (bf16[768,2048]{1,0:T(8,128)(2,1)S(1)}, bf16[768,2048]{1,0:T(8,128)(2,1)}, u32[]{:S(2)}) copy-start(bf16[768,2048]{1,0:T(8,128)(2,1)} %param.7) | copy-start | bytes 9437188
  114.3 0.7 copy-start.5
  172.3 51.3 %all-to-all-start.1 = ((bf16[16,256,256]{2,1,0:T(8,128)(2,1)}), bf16[16,256,256]{2,1,0:T(8,128)(2,1)S(1)}, u32[]{:S(2)}, u32[]{:S(2)}) async-start(bf16[16,256,256]{2,1,0:T(8,128)(2,1)} %get-tuple-element.4), calls=%async_computation.1 | async-start | bytes 4194304 | tf_op jit(solution)/shard_map/all_to_all | solution.py:17
  175.9 118.2 %all-gather.5.cloned.1.call-start = ((), (), s32[]{:S(2)}) async-start(), calls=%async_computation.6 | async-start | bytes 7864320 | tf_op jit(solution)/shard_map/all_gather | solution.py:56
  225.1 7.2 %copy-start.2 = (bf16[8,2,256,256]{3,2,0,1:T(8,128)(2,1)S(1)}, bf16[8,2,256,256]{3,2,0,1:T(8,128)(2,1)}, u32[]{:S(2)}) copy-start(bf16[8,2,256,256]{3,2,0,1:T(8,128)(2,1)} %copy.31) | copy-start | bytes 6291460
  225.1 9.4 %copy-start.6 = (bf16[2,1536,2048]{2,1,0:T(8,128)(2,1)S(1)}, bf16[2,1536,2048]{2,1,0:T(8,128)(2,1)}, u32[]{:S(2)}) copy-start(bf16[2,1536,2048]{2,1,0:T(8,128)(2,1)} %all-gather.3.cloned.1.call-done) | copy-start | bytes 37748740
  294.1 7.4 %copy-start.3 = (bf16[8,2,128,512]{3,2,0,1:T(8,128)(2,1)}, bf16[8,2,128,512]{3,2,0,1:T(8,128)(2,1)S(1)}, u32[]{:S(2)}) copy-start(bf16[8,2,128,512]{3,2,0,1:T(8,128)(2,1)S(1)} %copy.32) | copy-start | bytes 6291460
  315.9 4.0 copy-start.4
  315.9 74.2 %all-to-all-start.4 = ((bf16[2,1536,512]{2,0,1:T(2,128)(2,1)}), bf16[2,1536,512]{2,0,1:T(2,128)(2,1)S(1)}, u32[]{:S(2)}, u32[]{:S(2)}) async-start(bf16[2,1536,512]{2,0,1:T(2,128)(2,1)} %copy.33), calls=%async_computation.4 | async-start | bytes 6291456 | tf_op jit(solution)/shard_map/all_to_all | solution.py:60
  390.2 1.7 copy-start
Sparse Core Ops, SparseCore 0:
  114.5 81.0 all-gather.2
  239.7 46.2 all-gather.4
where the time goes:
time: 417 us; the launch traced here: 416 us
  blocking collectives  181 us (43%)
  waiting for transfers between devices  114 us (27%)
  local copies, waits for them, and re-layouts  51.1 us (12%)
  other arithmetic  27.5 us (7%)
  matrix products  19.5 us (5%)
  between operations  14.3 us (3%)
  starting transfers between devices  7.87 us (2%)
    all_to_all x1, blocking collectives, per_device(): lax.all_to_all(outbox.reshape(experts, capacity, column_width), 'fs', spl...  77.8 us
    all_to_all x1, waiting for transfers between devices, per_device(): lax.all_to_all(expert_out, 'fs', split_axis=1, concat_axis=0, tiled=True)  70 us
    all_to_all x1, blocking collectives, per_device(): lax.all_to_all(down_half, 'fs', split_axis=0, concat_axis=1, tiled=True)  51.8 us
    all_to_all x1, blocking collectives, per_device(): lax.all_to_all(up_half, 'fs', split_axis=0, concat_axis=1, tiled=True)  51.5 us
    all_to_all x1, waiting for transfers between devices, per_device(): lax.all_to_all(gate_half, 'fs', split_axis=0, concat_axis=1, tiled=True)  44.4 us
    convert_element_type x1, local copies, waits for them, and re-layouts, per_device(): expert_out = jnp.einsum('erf,efd->erd', lax.all_gather(hidden, 'tp', axis...  14.5 us
    scatter x1, local copies, waits for them, and re-layouts, per_device(): jnp.zeros((experts * capacity, column_width), jnp.bfloat16).at[slot_index]  8.85 us
  transfers between devices with their start and end apart: 4, of which 2 were waited for; matrix products, arithmetic and copies ran while one was open for 3% of the time, Pallas kernels for 0%

commit v1 on v0

--- a/solution.py
+++ b/solution.py
@@ -57,7 +57,10 @@
         down_new,
         preferred_element_type=jnp.float32,
     ).astype(jnp.bfloat16)
-    returned = lax.all_to_all(expert_out, "fs", split_axis=1, concat_axis=0, tiled=True)
+    returned = jnp.concatenate(
+        lax.all_to_all(jnp.stack(jnp.split(expert_out, lax.axis_size("fs"), axis=1)), "fs", 0, 0),
+        axis=0,
+    )
     picked = returned.reshape(experts * capacity, -1)[slot_index].reshape(
         token_count, top_count, -1
     )

time: 417 us -> 404 us (0.969)
  local copies, waits for them, and re-layouts: 51.1 us -> 38.7 us
    convert_element_type x1 -> x0, local copies, waits for them, and re-layouts: 14.5 us -> none  [per_device(): expert_out = jnp.einsum('erf,efd->erd', lax.all_gather(hidden, 'tp', axis...]
    unnamed x15 -> x20, local copies, waits for them, and re-layouts: 5.42 us -> 9.19 us
where the time goes in v1:
time: 404 us; the launch traced here: 403 us
  blocking collectives  181 us (45%)
  waiting for transfers between devices  115 us (28%)
  local copies, waits for them, and re-layouts  38.7 us (10%)
  other arithmetic  27.5 us (7%)
  matrix products  19.5 us (5%)
  between operations  14.3 us (4%)
  starting transfers between devices  7.65 us (2%)
    all_to_all x1, blocking collectives, per_device(): lax.all_to_all(outbox.reshape(experts, capacity, column_width), 'fs', spl...  77.8 us
    all_to_all x1, waiting for transfers between devices, per_device(): lax.all_to_all(jnp.stack(jnp.split(expert_out, lax.axis_size('fs'), axis=...  70.1 us
    all_to_all x1, blocking collectives, per_device(): lax.all_to_all(down_half, 'fs', split_axis=0, concat_axis=1, tiled=True)  51.8 us
    all_to_all x1, blocking collectives, per_device(): lax.all_to_all(up_half, 'fs', split_axis=0, concat_axis=1, tiled=True)  51.5 us
    all_to_all x1, waiting for transfers between devices, per_device(): lax.all_to_all(gate_half, 'fs', split_axis=0, concat_axis=1, tiled=True)  44.4 us
    unnamed x20, local copies, waits for them, and re-layouts  9.19 us
    scatter x1, local copies, waits for them, and re-layouts, per_device(): jnp.zeros((experts * capacity, column_width), jnp.bfloat16).at[slot_index]  8.85 us
  transfers between devices with their start and end apart: 4, of which 2 were waited for; matrix products, arithmetic and copies ran while one was open for 3% of the time, Pallas kernels for 0%

profile of v1, /device:TPU:0, one launch (start us, length us, event | category | flops | bytes accessed | tf_op | source)
XLA Modules:
  0.0 403.2 jit_solution(7655566963947066297)
XLA Ops:
  7.2 0.0 all-gather.3.cloned.1.call-start
  7.2 0.7 broadcast_multiply_fusion
  7.9 0.9 copy.17
  8.8 0.2 eq.29
  9.0 0.2 eq.25
  9.2 5.5 %convert_element_type.36 = f32[768,2048]{1,0:T(8,128)} convert(bf16[768,2048]{1,0:T(8,128)(2,1)} %param.7) | non-fusion elementwise | flops 1572864 | bytes 9437184 | tf_op jit(solution)/shard_map/convert_element_type | solution.py:29
  14.8 0.7 multiply_reduce_fusion
  15.5 0.2 copy.16
  15.7 0.3 mul.65
  15.9 4.5 %reduce-window.6 = s32[16,12,128]{2,1,0:T(8,128)S(1)} reduce-window(s32[16,12,128]{2,1,0:T(8,128)S(1)} %fusion.12, s32[]{:T(128)} %constant.15.clone.1), window={size=1x1x128 pad=0_0x0_0x127_0}, to_apply=%region_1.2 | reduce-window | flops 3121152 | bytes 196612 | tf_op jit(solution)/shard_map/reduce-window
  20.5 0.4 slice_reduce_fusion
  20.9 0.2 reduce-window.9
  21.1 0.1 broadcast_add_fusion
  21.3 1.6 fusion.1
  22.9 0.8 broadcast_in_dim.5
  23.7 2.0 reshape.96
  25.7 8.8 %scatter_custom_fusion = bf16[3072,512]{1,0:T(8,128)(2,1)S(1)} fusion(s32[1536]{0:T(1024)S(1)} %fusion.15, bf16[1536,512]{1,0:T(8,128)(2,1)} %reshape.96, bf16[]{:T(256)} %constant.13.clone.1), kind=kCustom, calls=%fused_computation.11 | custom fusion | bytes 3146240 | tf_op jit(solution)/shard_map/scatter | solution.py:41
  34.6 77.8 %all_to_all.77 = bf16[16,192,512]{2,1,0:T(8,128)(2,1)S(1)} all-to-all(bf16[16,192,512]{2,1,0:T(8,128)(2,1)S(1)} %bitcast.72), channel_id=1, replica_groups=mesh['fs'=8,'tp'=4] {'fs'}, dimensions={0} | all-to-all | bytes 6291456 | tf_op jit(solution)/shard_map/all_to_all | solution.py:43
  112.4 1.9 copy.19
  114.4 0.7 copy-done.4
  115.0 5.8 %multiply_convert_fusion.1 = (bf16[16,256,256]{2,1,0:T(8,128)(2,1)}, bf16[16,256,256]{2,1,0:T(8,128)(2,1)S(1)}) fusion(f32[16,256,256]{2,1,0:T(8,128)} %param.11, f32[256]{0:T(256)S(1)} %copy-done.4, f32[16,256,256]{2,1,0:T(8,128)} %param.12), kind=kLoop, calls=%fused_computation.4 | loop fusion | flops 4194304 | bytes 12583936 | tf_op jit(solution)/shard_map/convert_element_type | solution.py:13
  120.8 51.5 %all_to_all.78 = bf16[16,256,256]{2,1,0:T(8,128)(2,1)} all-to-all(bf16[16,256,256]{2,1,0:T(8,128)(2,1)S(1)} %get-tuple-element.5), channel_id=1, replica_groups=mesh['fs'=8,'tp'=4] {'fs'}, dimensions={0} | all-to-all | bytes 4194304 | tf_op jit(solution)/shard_map/all_to_all | solution.py:18
  172.3 3.6 all-to-all-start.1
  175.9 0.2 all-gather.5.cloned.1.call-start
  176.2 3.1 copy.21
  179.2 44.4 %all-to-all-done.1 = bf16[16,256,256]{2,1,0:T(8,128)(2,1)S(1)} async-done(((bf16[16,256,256]{2,1,0:T(8,128)(2,1)}), bf16[16,256,256]{2,1,0:T(8,128)(2,1)S(1)}, u32[]{:S(2)}, u32[]{:S(2)}) %all-to-all-start.1) | async-done | bytes 2097184 | tf_op jit(solution)/shard_map/all_to_all | solution.py:17
  223.6 1.5 copy.20
  225.1 7.2 %fusion.16 = f32[2,1536,256]{2,1,0:T(8,128)S(1)} fusion(bf16[2,1536,2048]{2,1,0:T(8,128)(2,1)} %all-gather.3.cloned.1.call-done, bf16[2,2048,256]{2,1,0:T(8,128)(2,1)} %bitcast.79), kind=kOutput, calls=%fused_computation.44 | convolution fusion | flops 3221225472 | bytes 17825792 | tf_op jit(solution)/shard_map/erd,edf->erf/dot_general | solution.py:51
  232.3 2.2 copy-done.5
  234.5 5.0 %fusion = bf16[2,1536,256]{2,1,0:T(8,128)(2,1)} fusion(bf16[2,1536,2048]{2,1,0:T(8,128)(2,1)S(1)} %copy-done.5, bf16[2,2048,256]{2,1,0:T(8,128)(2,1)S(1)} %bitcast.78, f32[2,1536,256]{2,1,0:T(8,128)S(1)} %fusion.16), kind=kOutput, calls=%fused_computation.8 | convolution fusion | flops 3225944064 | bytes 19398656 | tf_op jit(solution)/shard_map/erd,edf->erf/dot_general | solution.py:52
  239.6 2.5 convert_element_type.41
  242.1 51.8 %all_to_all.79 = bf16[16,128,512]{2,1,0:T(8,128)(2,1)S(1)} all-to-all(bf16[16,128,512]{2,1,0:T(8,128)(2,1)S(1)} %convert_element_type.41), channel_id=1, replica_groups=mesh['fs'=8,'tp'=4] {'fs'}, dimensions={0} | all-to-all | bytes 4194304 | tf_op jit(solution)/shard_map/all_to_all | solution.py:19
  293.9 0.2 copy.22
  294.1 7.3 %convolution_convert_fusion = bf16[2,1536,512]{2,1,0:T(8,128)(2,1)S(1)} fusion(bf16[2,1536,1024]{2,1,0:T(8,128)(2,1)} %all-gather.5.cloned.1.call-done, bf16[2,1024,512]{2,1,0:T(8,128)(2,1)S(1)} %bitcast.81), kind=kOutput, calls=%fused_computation.5 | convolution fusion | flops 3222798336 | bytes 11534336 | tf_op jit(solution)/shard_map/erf,efd->erd/dot_general | solution.py:54
  301.4 0.8 fusion.11
  302.2 0.8 fusion.10
  303.0 0.8 fusion.9
  303.7 0.8 fusion.8
  304.5 0.8 fusion.7
  305.3 0.8 fusion.6
  306.1 0.8 fusion.5
  306.9 0.8 fusion.4
  307.7 3.8 all-to-all-start.4
  311.5 0.2 copy.15
  311.7 70.1 %all-to-all-done.4 = bf16[8,2,192,512]{3,2,1,0:T(8,128)(2,1)S(1)} async-done(((bf16[8,2,192,512]{3,2,1,0:T(8,128)(2,1)}), bf16[8,2,192,512]{3,2,1,0:T(8,128)(2,1)S(1)}, u32[]{:S(2)}, u32[]{:S(2)}) %all-to-all-start.4) | async-done | bytes 3145760 | tf_op jit(solution)/shard_map/all_to_all | solution.py:61
  381.8 5.4 %gather_fusion = bf16[1536,512]{1,0:T(8,128)(2,1)} fusion(bf16[3072,512]{1,0:T(8,128)(2,1)S(1)} %bitcast.70, s32[2048]{0:T(1024)S(1)} %pad_clamp_fusion), kind=kCustom, calls=%fused_computation | custom fusion | bytes 3151872 | tf_op jit(solution)/shard_map/gather | solution.py:64
  387.2 3.4 reshape.83
  390.6 5.7 %multiply_reduce_fusion.1 = bf16[768,512]{1,0:T(8,128)(2,1)} fusion(f32[768,2,512]{2,1,0:T(2,128)S(1)} %reshape.83, f32[768,2]{1,0:T(8,128)S(1)} %copy.15), kind=kLoop, calls=%fused_computation.7 | loop fusion | flops 1179648 | bytes 3938304 | tf_op jit(solution)/shard_map/reduce_sum | solution.py:68
  (22 shorter events, 0.2 us)
Async XLA Ops:
  7.2 217.9 %all-gather.3.cloned.1.call-start = ((), (), s32[]{:S(2)}) async-start(), calls=%async_computation.5 | async-start | bytes 15728640 | tf_op jit(solution)/shard_map/all_gather | solution.py:50
  9.2 5.6 %copy-start = (bf16[768,2048]{1,0:T(8,128)(2,1)S(1)}, bf16[768,2048]{1,0:T(8,128)(2,1)}, u32[]{:S(2)}) copy-start(bf16[768,2048]{1,0:T(8,128)(2,1)} %param.7) | copy-start | bytes 9437188
  114.3 0.7 copy-start.4
  172.3 51.3 %all-to-all-start.1 = ((bf16[16,256,256]{2,1,0:T(8,128)(2,1)}), bf16[16,256,256]{2,1,0:T(8,128)(2,1)S(1)}, u32[]{:S(2)}, u32[]{:S(2)}) async-start(bf16[16,256,256]{2,1,0:T(8,128)(2,1)} %get-tuple-element.4), calls=%async_computation.1 | async-start | bytes 4194304 | tf_op jit(solution)/shard_map/all_to_all | solution.py:17
  175.9 118.2 %all-gather.5.cloned.1.call-start = ((), (), s32[]{:S(2)}) async-start(), calls=%async_computation.6 | async-start | bytes 7864320 | tf_op jit(solution)/shard_map/all_gather | solution.py:56
  225.1 7.2 %copy-start.1 = (bf16[8,2,256,256]{3,2,0,1:T(8,128)(2,1)S(1)}, bf16[8,2,256,256]{3,2,0,1:T(8,128)(2,1)}, u32[]{:S(2)}) copy-start(bf16[8,2,256,256]{3,2,0,1:T(8,128)(2,1)} %copy.21) | copy-start | bytes 6291460
  225.1 9.4 %copy-start.5 = (bf16[2,1536,2048]{2,1,0:T(8,128)(2,1)S(1)}, bf16[2,1536,2048]{2,1,0:T(8,128)(2,1)}, u32[]{:S(2)}) copy-start(bf16[2,1536,2048]{2,1,0:T(8,128)(2,1)} %all-gather.3.cloned.1.call-done) | copy-start | bytes 37748740
  294.1 7.4 %copy-start.2 = (bf16[8,2,128,512]{3,2,0,1:T(8,128)(2,1)}, bf16[8,2,128,512]{3,2,0,1:T(8,128)(2,1)S(1)}, u32[]{:S(2)}) copy-start(bf16[8,2,128,512]{3,2,0,1:T(8,128)(2,1)S(1)} %copy.22) | copy-start | bytes 6291460
  307.7 3.8 copy-start.3
  307.7 74.1 %all-to-all-start.4 = ((bf16[8,2,192,512]{3,2,1,0:T(8,128)(2,1)}), bf16[8,2,192,512]{3,2,1,0:T(8,128)(2,1)S(1)}, u32[]{:S(2)}, u32[]{:S(2)}) async-start(bf16[8,2,192,512]{3,2,1,0:T(8,128)(2,1)} %fusion.4), calls=%async_computation.4 | async-start | bytes 6291456 | tf_op jit(solution)/shard_map/all_to_all | solution.py:61
Sparse Core Ops, SparseCore 0:
  114.5 81.0 all-gather.2
  239.7 46.2 all-gather.4
